TPU v7x, 32 devices: a whole 2x2x4 slice. The times are simulated.
32 devices in a mesh: ep: 16 (over z, y, x), tp: 2 (over core).
Axes of the slice: x: 2, y: 2, z: 4, core: 2. Of those that a mesh axis runs over, the one named last changes fastest.
Arguments:
- tokens: bfloat16 [6144, 3072], P('ep', 'tp'), may hold values from -6 to 6
- cotangent: bfloat16 [6144, 3072], P('ep', 'tp'), may hold values from -6 to 6
- experts: int32 [6144, 2], P('ep'), may hold values from 0 to 15, all different within a row; in each aligned block of 384 rows (0 to 383, 384 to 767, ...) at most 72 rows name the same one
- gate: float32 [6144, 2], P('ep'), may hold values from 0.2 to 1
- w_gate: bfloat16 [16, 3072, 768], P('ep', None, 'tp'), may hold values from -0.109375 to 0.109375
- w_up: bfloat16 [16, 3072, 768], P('ep', None, 'tp'), may hold values from -0.109375 to 0.109375
- w_down: bfloat16 [16, 768, 3072], P('ep', 'tp'), may hold values from -0.21875 to 0.21875
Outputs:
- token_grad: bfloat16 [6144, 3072], P('ep', 'tp')
- gate_grad: float32 [6144, 2], P('ep')
- gate_weight_grad: bfloat16 [16, 3072, 768], P('ep', None, 'tp')
- up_weight_grad: bfloat16 [16, 3072, 768], P('ep', None, 'tp')
- down_weight_grad: bfloat16 [16, 768, 3072], P('ep', 'tp')
- gate_row_norms: float32 [16, 3072], P('ep')
- up_row_norms: float32 [16, 3072], P('ep')
- down_row_norms: float32 [16, 768], P('ep', 'tp')
Inputs may be any that keep to these rules, and one draw needn't show every extreme that they name: A row names 2 different experts. In each aligned block of 384 rows (the rows of one index of ep) no expert is named by more than 72 rows, a bound that some block reaches.
All inputs are finite; a program needn't handle non-finite values.
Results may differ from a plain program's by a relative error of at most 0.008.
Values may be sent and summed in bfloat16 or wider, within the bound.
A program may use at most 128 MiB of HBM per device.

v0:
```python
import jax
import jax.numpy as jnp
from jax import lax
from jax.sharding import PartitionSpec as P


def slot_table(route_block, experts_count, cap):
    pair_ids = route_block.reshape(-1)
    pair_count = pair_ids.shape[0]
    onehot = (pair_ids[:, None] == jnp.arange(experts_count, dtype=jnp.int32)[None, :]).astype(
        jnp.int32
    )
    ranking = jnp.sum(jnp.cumsum(onehot, axis=0) * onehot, axis=1) - 1
    slot_of = pair_ids * cap + ranking
    slot_pairs = (
        jnp.full((experts_count * cap,), pair_count, jnp.int32)
        .at[slot_of]
        .set(jnp.arange(pair_count, dtype=jnp.int32))
    )
    return (slot_of, slot_pairs)


def per_device(tokens, cotangent, experts, gate, w_gate, w_up, w_down):
    groups = lax.axis_size("ep")
    tok_rows, top = experts.shape
    cap = 3 * tok_rows * top // (2 * groups)
    slot_of, slot_pairs = slot_table(experts, groups, cap)
    token_of = slot_pairs // top
    cols = tokens.shape[1]
    weighted = (gate[:, :, None] * cotangent.astype(jnp.float32)[:, None, :]).astype(jnp.bfloat16)
    padding = jnp.zeros((1, cols), jnp.bfloat16)
    sent_tok = jnp.concatenate([tokens, padding], axis=0)[token_of].reshape(groups, cap, cols)
    sent_cot = jnp.concatenate([weighted.reshape(-1, cols), padding], axis=0)[slot_pairs]
    sent_tok, sent_cot = (sent_tok, sent_cot.reshape(groups, cap, cols))
    half_tok, half_cot = (
        lax.all_to_all(sent_tok, "ep", split_axis=0, concat_axis=0, tiled=True),
        lax.all_to_all(sent_cot, "ep", split_axis=0, concat_axis=0, tiled=True),
    )
    recv_tok, recv_cot = (
        lax.all_gather(half_tok, "tp", axis=2, tiled=True),
        lax.all_gather(half_cot, "tp", axis=2, tiled=True),
    )
    cols = recv_tok.shape[2]
    rows_in = recv_tok.reshape(-1, cols)
    rows_cot = recv_cot.reshape(-1, cols)
    gate_mat = w_gate[0]
    up_mat = w_up[0]
    down_mat = w_down[0]
    contract_last = (((1,), (1,)), ((), ()))
    contract_rows = (((0,), (0,)), ((), ()))
    gate_pre = jnp.dot(rows_in, gate_mat, preferred_element_type=jnp.float32)
    up_pre = jnp.dot(rows_in, up_mat, preferred_element_type=jnp.float32)
    sigma = jax.nn.sigmoid(gate_pre)
    active = gate_pre * sigma
    hidden = (active * up_pre).astype(jnp.bfloat16)
    hidden_grad = lax.dot_general(
        rows_cot, down_mat, contract_last, preferred_element_type=jnp.float32
    )
    product_part = jnp.sum(hidden.astype(jnp.float32) * hidden_grad, axis=1)
    gate_grad_pre = (hidden_grad * up_pre * sigma * (1.0 + gate_pre * (1.0 - sigma))).astype(
        jnp.bfloat16
    )
    up_grad_pre = (hidden_grad * active).astype(jnp.bfloat16)
    partial_rows = lax.dot_general(
        gate_grad_pre, gate_mat, contract_last, preferred_element_type=jnp.float32
    )
    partial_rows = partial_rows + lax.dot_general(
        up_grad_pre, up_mat, contract_last, preferred_element_type=jnp.float32
    )
    row_grads = lax.psum_scatter(
        partial_rows.astype(jnp.bfloat16), "tp", scatter_dimension=1, tiled=True
    )
    products = lax.psum(product_part, "tp").astype(jnp.bfloat16)
    back_rows, back_products = (
        lax.all_to_all(
            row_grads.reshape(groups, cap, -1), "ep", split_axis=0, concat_axis=0, tiled=True
        ),
        lax.all_to_all(
            products.reshape(groups, cap), "ep", split_axis=0, concat_axis=0, tiled=True
        ),
    )
    half_cols = back_rows.shape[2]
    pair_rows = (
        back_rows.reshape(-1, half_cols)[slot_of]
        .astype(jnp.float32)
        .reshape(tok_rows, top, half_cols)
    )
    token_grad = jnp.sum(pair_rows, axis=1).astype(jnp.bfloat16)
    gate_grad = back_products.reshape(-1)[slot_of].astype(jnp.float32).reshape(tok_rows, top) / gate
    gate_sum = lax.dot_general(
        rows_in, gate_grad_pre, contract_rows, preferred_element_type=jnp.float32
    )
    up_sum = lax.dot_general(
        rows_in, up_grad_pre, contract_rows, preferred_element_type=jnp.float32
    )
    down_sum = lax.dot_general(hidden, rows_cot, contract_rows, preferred_element_type=jnp.float32)
    gate_norms, up_norms = lax.psum(
        (jnp.sum(gate_sum * gate_sum, axis=1), jnp.sum(up_sum * up_sum, axis=1)), "tp"
    )
    down_norms = jnp.sum(down_sum * down_sum, axis=1)
    return (
        token_grad,
        gate_grad,
        gate_sum.astype(jnp.bfloat16)[None],
        up_sum.astype(jnp.bfloat16)[None],
        down_sum.astype(jnp.bfloat16)[None],
        gate_norms[None],
        up_norms[None],
        down_norms[None],
    )


def solution(mesh):
    placed = (
        P("ep", "tp"),
        P("ep", "tp"),
        P("ep", None),
        P("ep", None),
        P("ep", None, "tp"),
        P("ep", None, "tp"),
        P("ep", "tp", None),
    )
    return jax.shard_map(
        per_device,
        mesh=mesh,
        in_specs=placed,
        out_specs=(
            P("ep", "tp"),
            P("ep", None),
            P("ep", None, "tp"),
            P("ep", None, "tp"),
            P("ep", "tp", None),
            P("ep", None),
            P("ep", None),
            P("ep", "tp"),
        ),
        check_vma=False,
    )
```

profile of v0, /device:TPU:14, one launch (start us, length us, event | category | flops | bytes accessed | tf_op | source)
XLA Modules:
  0.0 402.0 jit_solution(8964741844496991647)
XLA Ops:
  7.2 0.8 broadcast_multiply_fusion
  8.0 0.8 copy.28
  8.8 0.1 eq.29
  9.0 0.1 eq.25
  9.1 0.1 copy.27
  9.3 0.2 mul.77
  9.5 1.7 reduce-window.6
  11.2 0.3 slice_reduce_fusion
  11.5 0.1 fusion.11
  11.6 3.4 scatter_custom_fusion
  15.0 2.4 concatenate.7
  17.4 10.2 %gather_fusion.1 = bf16[1152,1536]{1,0:T(8,128)(2,1)} fusion(bf16[385,1536]{1,0:T(8,128)(2,1)} %concatenate.7, s32[2048]{0:T(1024)S(1)} %get-tuple-element.47), kind=kCustom, calls=%fused_computation.1 | custom fusion | bytes 7082496 | tf_op jit(solution)/shard_map/gather | solution.py:32
  27.6 7.3 %all-to-all-start.1 = ((bf16[16,72,1536]{2,1,0:T(8,128)(2,1)}), bf16[16,72,1536]{2,1,0:T(8,128)(2,1)}, u32[]{:S(2)}, u32[]{:S(2)}) async-start(bf16[16,72,1536]{2,1,0:T(8,128)(2,1)} %bitcast.57), calls=%async_computation.1 | async-start | bytes 7077888 | tf_op jit(solution)/shard_map/all_to_all | solution.py:36
  34.9 0.1 copy.26
  35.1 0.1 mul.70
  35.2 4.7 %mul.72 = f32[384,2,1536]{2,1,0:T(2,128)} broadcast(bf16[384,1536]{1,0:T(8,128)(2,1)} %param.8), dimensions={0,2} | broadcast | bytes 5898240 | tf_op jit(solution)/shard_map/mul | solution.py:30
  39.9 6.7 %mul.73 = f32[768,1536]{1,0:T(8,128)} reshape(f32[384,2,1536]{2,1,0:T(2,128)} %mul.72) | data formatting | bytes 9437184 | tf_op jit(solution)/shard_map/mul | solution.py:30
  46.6 68.1 %all-to-all-done.1 = bf16[16,72,1536]{2,1,0:T(8,128)(2,1)} async-done(((bf16[16,72,1536]{2,1,0:T(8,128)(2,1)}), bf16[16,72,1536]{2,1,0:T(8,128)(2,1)}, u32[]{:S(2)}, u32[]{:S(2)}) %all-to-all-start.1) | async-done | bytes 3538976 | tf_op jit(solution)/shard_map/all_to_all | solution.py:36
  114.7 0.0 all-gather.3.cloned.1.call-start
  114.8 2.7 multiply_convert_fusion
  117.4 1.6 concatenate.6
  119.0 11.1 %gather_fusion = bf16[1152,1536]{1,0:T(8,128)(2,1)} fusion(bf16[769,1536]{1,0:T(8,128)(2,1)} %concatenate.6, s32[2048]{0:T(1024)S(1)} %get-tuple-element.48), kind=kCustom, calls=%fused_computation | custom fusion | bytes 7082496 | tf_op jit(solution)/shard_map/gather | solution.py:33
  130.1 82.0 %all_to_all.25 = bf16[16,72,1536]{2,1,0:T(8,128)(2,1)} all-to-all(bf16[16,72,1536]{2,1,0:T(8,128)(2,1)} %bitcast.58), channel_id=1, replica_groups=mesh['ep'=16,'tp'=2] {'ep'}, dimensions={0} | all-to-all | bytes 7077888 | tf_op jit(solution)/shard_map/all_to_all | solution.py:37
  212.1 0.2 reduce-scatter.2.cloned.1.call-start
  212.4 6.9 %fusion.2 = f32[1152,384]{0,1:T(8,128)} fusion(bf16[1152,3072]{1,0:T(8,128)(2,1)} %bitcast.65, bf16[1,3072,384]{2,1,0:T(8,128)(2,1)S(1)} %copy-done), kind=kOutput, calls=%fused_computation.12 | convolution fusion | flops 2717908992 | bytes 11206656 | tf_op jit(solution)/shard_map/dot_general | solution.py:51
  219.3 4.5 %fusion.5 = f32[1152,384]{0,1:T(8,128)} fusion(bf16[1152,3072]{1,0:T(8,128)(2,1)S(1)} %bitcast.68, bf16[1,3072,384]{2,1,0:T(8,128)(2,1)S(1)} %copy-done.2), kind=kOutput, calls=%fused_computation.15 | convolution fusion | flops 2717908992 | bytes 11206656 | tf_op jit(solution)/shard_map/dot_general | solution.py:52
  223.7 6.7 %all-gather.3.cloned.1.call-done = bf16[16,72,3072]{2,1,0:T(8,128)(2,1)} async-done(((bf16[16,72,1536]{2,1,0:T(8,128)(2,1)}), bf16[16,72,3072]{2,1,0:T(8,128)(2,1)}) %all-gather.3.cloned.1.call-update) | async-done | bytes 7077904 | tf_op jit(solution)/shard_map/all_gather | solution.py:41
  230.4 9.4 %multiply_reduce_fusion.3 = (f32[1152]{0:T(1024)S(1)}, bf16[1152,384]{0,1:T(8,128)(2,1)}, bf16[1152,384]{0,1:T(8,128)(2,1)S(1)}, bf16[1152,384]{0,1:T(8,128)(2,1)S(1)}) fusion(f32[1152,384]{0,1:T(8,128)} %fusion.5, f32[1152,384]{0,1:T(8,128)} %fusion.2, bf16[1152,3072]{1,0:T(8,128)(2,1)} %bitcast.63, bf16[1,384,3072]{2,1,0:T(8,128)(2,1)} %param.13), kind=kOutput, calls=%fused_computation.22 | convolution fusion | flops 2725870592 | bytes 15634944 | tf_op jit(solution)/shard_map/dot_general | solution.py:56
  239.9 7.1 %fusion = f32[1152,3072]{1,0:T(8,128)} fusion(bf16[1152,384]{0,1:T(8,128)(2,1)S(1)} %get-tuple-element.37, bf16[1,3072,384]{2,1,0:T(8,128)(2,1)S(1)} %copy-done), kind=kOutput, calls=%fused_computation.10 | convolution fusion | flops 2717908992 | bytes 17399808 | tf_op jit(solution)/shard_map/dot_general | solution.py:64
  246.9 8.9 %add_convert_fusion = bf16[1152,3072]{1,0:T(8,128)(2,1)} fusion(f32[1152,3072]{1,0:T(8,128)} %fusion, bf16[1152,384]{0,1:T(8,128)(2,1)S(1)} %get-tuple-element.44, bf16[1,3072,384]{2,1,0:T(8,128)(2,1)S(1)} %copy-done.3), kind=kOutput, calls=%fused_computation.5 | convolution fusion | flops 2724986880 | bytes 24477696 | tf_op jit(solution)/shard_map/dot_general | solution.py:67
  255.9 6.7 %convert_bitcast_fusion.2 = (bf16[1,3072,384]{1,2,0:T(8,128)(2,1)S(1)}, f32[3072]{0:T(1024)S(1)}) fusion(bf16[1152,384]{0,1:T(8,128)(2,1)S(1)} %get-tuple-element.37, bf16[1152,3072]{1,0:T(8,128)(2,1)} %bitcast.66), kind=kOutput, calls=%fused_computation.21 | convolution fusion | flops 2721444864 | bytes 10334208 | tf_op jit(solution)/shard_map/dot_general | solution.py:90
  262.7 8.3 %convert_bitcast_fusion.1 = (bf16[1,3072,384]{1,2,0:T(8,128)(2,1)}, f32[3072]{0:T(1024)S(1)}) fusion(bf16[1152,384]{0,1:T(8,128)(2,1)S(1)} %copy-done.5, bf16[1152,3072]{1,0:T(8,128)(2,1)} %bitcast.67), kind=kOutput, calls=%fused_computation.20 | convolution fusion | flops 2721444864 | bytes 10334208 | tf_op jit(solution)/shard_map/dot_general | solution.py:93
  271.0 4.0 all-reduce.2
  274.9 0.1 all_to_all.20
  275.0 10.9 %all_to_all.26 = bf16[16,1,72]{2,1,0:T(2,128)(2,1)S(1)} all-to-all(bf16[16,1,72]{2,1,0:T(2,128)(2,1)S(1)} %all_to_all.20), channel_id=1, replica_groups=mesh['ep'=16,'tp'=2] {'ep'}, dimensions={0} | all-to-all | bytes 4608 | tf_op jit(solution)/shard_map/all_to_all | solution.py:78
  286.0 7.5 %all-to-all-start.2 = ((bf16[16,72,1536]{2,1,0:T(8,128)(2,1)}), bf16[16,72,1536]{2,1,0:T(8,128)(2,1)}, u32[]{:S(2)}, u32[]{:S(2)}) async-start(bf16[16,72,1536]{2,1,0:T(8,128)(2,1)} %bitcast.59), calls=%async_computation.3 | async-start | bytes 7077888 | tf_op jit(solution)/shard_map/all_to_all | solution.py:75
  293.5 7.9 %multiply_reduce_fusion = (f32[384]{0:T(512)S(1)}, bf16[1,384,3072]{2,1,0:T(8,128)(2,1)}) fusion(bf16[1152,384]{0,1:T(8,128)(2,1)} %get-tuple-element.36, bf16[1152,3072]{1,0:T(8,128)(2,1)} %bitcast.64), kind=kOutput, calls=%fused_computation.6 | convolution fusion | flops 2721447424 | bytes 10323456 | tf_op jit(solution)/shard_map/dot_general | solution.py:96
  301.4 0.6 broadcast_in_dim.42
  302.0 4.3 %copy.35 = bf16[1,3072,384]{2,1,0:T(8,128)(2,1)} copy(bf16[1,3072,384]{1,2,0:T(8,128)(2,1)} %get-tuple-element.40) | data formatting | bytes 4718592
  306.2 2.4 copy.34
  308.7 0.1 reshape.112
  308.8 5.0 %gather_fusion.3 = bf16[768]{0:T(1024)(128)(2,1)S(1)} fusion(bf16[1152]{0:T(1024)(128)(2,1)S(1)} %reshape.112, s32[1024]{0:T(1024)S(1)} %pad_clamp_fusion.2), kind=kCustom, calls=%fused_computation.3 | custom fusion | bytes 6144 | tf_op jit(solution)/shard_map/gather | solution.py:89
  313.8 0.2 reshape.113
  314.0 0.7 copy.33
  314.7 57.3 %all-to-all-done.2 = bf16[16,72,1536]{2,1,0:T(8,128)(2,1)} async-done(((bf16[16,72,1536]{2,1,0:T(8,128)(2,1)}), bf16[16,72,1536]{2,1,0:T(8,128)(2,1)}, u32[]{:S(2)}, u32[]{:S(2)}) %all-to-all-start.2) | async-done | bytes 3538976 | tf_op jit(solution)/shard_map/all_to_all | solution.py:75
  372.0 8.4 %gather_fusion.2 = bf16[768,1536]{1,0:T(8,128)(2,1)} fusion(bf16[1152,1536]{1,0:T(8,128)(2,1)} %bitcast.9, s32[1024]{0:T(1024)S(1)} %pad_clamp_fusion.2), kind=kCustom, calls=%fused_computation.2 | custom fusion | bytes 4721664 | tf_op jit(solution)/shard_map/gather | solution.py:84
  380.4 6.2 %gather.17 = bf16[384,2,1536]{2,1,0:T(2,128)(2,1)} reshape(bf16[768,1536]{1,0:T(8,128)(2,1)} %gather_fusion.2) | data formatting | bytes 4718592 | tf_op jit(solution)/shard_map/gather | solution.py:84
  386.6 8.4 %reduce_sum.58 = bf16[384,1536]{1,0:T(8,128)(2,1)} reduce(bf16[384,2,1536]{2,1,0:T(2,128)(2,1)} %gather.17, bf16[]{:T(256)} %constant.13.clone.1), dimensions={1}, to_apply=%region_5.6 | reduce | flops 589824 | bytes 3538946 | tf_op jit(solution)/shard_map/reduce_sum | solution.py:88
  (32 shorter events, 0.3 us)
Async XLA Ops:
  7.2 205.2 %copy-start = (bf16[1,3072,384]{2,1,0:T(8,128)(2,1)S(1)}, bf16[1,3072,384]{2,1,0:T(8,128)(2,1)}, u32[]{:S(2)}) copy-start(bf16[1,3072,384]{2,1,0:T(8,128)(2,1)} %param.11) | copy-start | bytes 7077892
  27.6 7.3 %copy-start.6 = (f32[384,2]{0,1:T(2,128)S(1)}, f32[384,2]{0,1:T(2,128)}, u32[]{:S(2)}) copy-start(f32[384,2]{0,1:T(2,128)} %param.10) | copy-start | bytes 9220
  27.6 87.1 %all-to-all-start.1 = ((bf16[16,72,1536]{2,1,0:T(8,128)(2,1)}), bf16[16,72,1536]{2,1,0:T(8,128)(2,1)}, u32[]{:S(2)}, u32[]{:S(2)}) async-start(bf16[16,72,1536]{2,1,0:T(8,128)(2,1)} %bitcast.57), calls=%async_computation.1 | async-start | bytes 7077888 | tf_op jit(solution)/shard_map/all_to_all | solution.py:36
  34.9 177.5 %all-gather.5.cloned.1.call-start = ((), (), s32[]{:S(2)}) async-start(), calls=%async_computation.6 | async-start | bytes 10616832 | tf_op jit(solution)/shard_map/all_gather | solution.py:40
  114.7 115.7 %all-gather.3.cloned.1.call-start = ((), (), s32[]{:S(2)}) async-start(), calls=%async_computation.5 | async-start | bytes 10616832 | tf_op jit(solution)/shard_map/all_gather | solution.py:41
  212.1 73.9 %reduce-scatter.2.cloned.1.call-start = ((), (), s32[]{:S(2)}) async-start(), calls=%async_computation.7 | async-start | bytes 10616832 | tf_op jit(solution)/shard_map/reduce_scatter | solution.py:70
  212.4 6.9 %copy-start.2 = (bf16[1,3072,384]{2,1,0:T(8,128)(2,1)S(1)}, bf16[1,3072,384]{2,1,0:T(8,128)(2,1)}, u32[]{:S(2)}) copy-start(bf16[1,3072,384]{2,1,0:T(8,128)(2,1)} %param.12) | copy-start | bytes 7077892
  212.4 6.9 %copy-start.7 = (bf16[16,72,3072]{2,1,0:T(8,128)(2,1)S(1)}, bf16[16,72,3072]{2,1,0:T(8,128)(2,1)}, u32[]{:S(2)}) copy-start(bf16[16,72,3072]{2,1,0:T(8,128)(2,1)} %all-gather.5.cloned.1.call-done) | copy-start | bytes 21233668
  239.9 7.1 %copy-start.4 = (bf16[1152,384]{0,1:T(8,128)(2,1)}, bf16[1152,384]{0,1:T(8,128)(2,1)S(1)}, u32[]{:S(2)}) copy-start(bf16[1152,384]{0,1:T(8,128)(2,1)S(1)} %get-tuple-element.44) | copy-start | bytes 2654212
  239.9 7.1 %copy-start.3 = (bf16[1,3072,384]{2,1,0:T(8,128)(2,1)S(1)}, bf16[1,3072,384]{2,1,0:T(8,128)(2,1)}, u32[]{:S(2)}) copy-start(bf16[1,3072,384]{2,1,0:T(8,128)(2,1)} %param.12) | copy-start | bytes 7077892
  255.9 6.7 %copy-start.5 = (bf16[1152,384]{0,1:T(8,128)(2,1)S(1)}, bf16[1152,384]{0,1:T(8,128)(2,1)}, u32[]{:S(2)}) copy-start(bf16[1152,384]{0,1:T(8,128)(2,1)} %copy-done.4) | copy-start | bytes 2654212
  286.0 86.1 %all-to-all-start.2 = ((bf16[16,72,1536]{2,1,0:T(8,128)(2,1)}), bf16[16,72,1536]{2,1,0:T(8,128)(2,1)}, u32[]{:S(2)}, u32[]{:S(2)}) async-start(bf16[16,72,1536]{2,1,0:T(8,128)(2,1)} %bitcast.59), calls=%async_computation.3 | async-start | bytes 7077888 | tf_op jit(solution)/shard_map/all_to_all | solution.py:75
  380.4 14.6 %copy-start.1 = (bf16[1,3072,384]{2,1,0:T(8,128)(2,1)S(1)}, bf16[1,3072,384]{2,1,0:T(8,128)(2,1)}, u32[]{:S(2)}) copy-start(bf16[1,3072,384]{2,1,0:T(8,128)(2,1)} %param.11) | copy-start | bytes 7077892
Sparse Core Ops, SparseCore 0:
  114.8 17.2 all-gather.4
  212.2 18.1 all-gather.2
  256.0 15.8 reduce-scatter.1
where the time goes:
time: 410 us; the launch traced here: 402 us
  waiting for transfers between devices  132 us (32%)
  blocking collectives  96.9 us (24%)
  local copies, waits for them, and re-layouts  69.8 us (17%)
  matrix products  59.8 us (15%)
  starting transfers between devices  15.1 us (4%)
  between operations  14.4 us (4%)
  other arithmetic  13.9 us (3%)
    all_to_all x1, blocking collectives, per_device(): lax.all_to_all(sent_cot, 'ep', split_axis=0, concat_axis=0, tiled=True)  82 us
    all_to_all x1, waiting for transfers between devices, per_device(): lax.all_to_all(sent_tok, 'ep', split_axis=0, concat_axis=0, tiled=True)  68.1 us
    all_to_all x1, waiting for transfers between devices, per_device(): lax.all_to_all(row_grads.reshape(groups, cap, -1), 'ep', split_axis=0, co...  57.3 us
    gather x2, local copies, waits for them, and re-layouts, per_device(): back_rows.reshape(-1, half_cols)[slot_of].astype(jnp.float32)  14.6 us
    mul x3, local copies, waits for them, and re-layouts, per_device(): gate[:, :, None] * cotangent.astype(jnp.float32)[:, None, :]  11.5 us
    gather x1, local copies, waits for them, and re-layouts, per_device(): jnp.concatenate([weighted.reshape(-1, cols), padding], axis=0)[slot_pairs]  11.1 us
    all_to_all x1, blocking collectives, per_device(): lax.all_to_all(products.reshape(groups, cap), 'ep', split_axis=0, concat_...  10.9 us
    gather x1, local copies, waits for them, and re-layouts, per_device(): jnp.concatenate([tokens, padding], axis=0)[token_of]  10.2 us
  transfers between devices with their start and end apart: 5, of which 3 were waited for; matrix products, arithmetic and copies ran while one was open for 19% of the time, Pallas kernels for 0%

commit v1 on v0

v1 whole, which is shorter than its diff:
```python
import jax
import jax.numpy as jnp
from jax import lax
from jax.sharding import PartitionSpec as P

F32 = jnp.float32
BF16 = jnp.bfloat16
LAST = (((1,), (1,)), ((), ()))
ROWS = (((0,), (0,)), ((), ()))


def slots_of(routes, groups, cap):
    rows = routes.shape[1]
    ids = lax.broadcasted_iota(jnp.int32, (groups, rows), 0)
    hits = [routes[k][None, :] == ids for k in range(routes.shape[0])]
    named = sum(h.astype(F32) for h in hits).astype(BF16)
    before = (
        lax.broadcasted_iota(jnp.int32, (rows, rows), 0)
        < lax.broadcasted_iota(jnp.int32, (rows, rows), 1)
    ).astype(BF16)
    rank = jnp.dot(named, before, preferred_element_type=F32)
    return jnp.stack(
        [routes[k] * cap + jnp.sum(jnp.where(h, rank, 0.0), axis=0).astype(jnp.int32) for k, h in enumerate(hits)]
    )


def per_device(tokens, cotangent, experts, gate, w_gate, w_up, w_down):
    groups = lax.axis_size("ep")
    tok_rows, top = experts.shape
    cap = 3 * tok_rows * top // (2 * groups)
    total = groups * cap
    half = tokens.shape[1]
    core = lax.axis_index("tp")
    swap = [(0, 1), (1, 0)]
    slot = slots_of(experts.T, groups, cap)
    gate_t = gate.T
    slot_ids = lax.broadcasted_iota(jnp.int32, (total, tok_rows), 0)
    match = [slot[k][None, :] == slot_ids for k in range(top)]
    pick = sum(m.astype(F32) for m in match).astype(BF16)
    slot_gate = sum(
        jnp.sum(jnp.where(m, gate_t[k][None, :], 0.0), axis=1, keepdims=True) for k, m in enumerate(match)
    )
    pick, slot_gate = lax.optimization_barrier((pick, slot_gate))

    def exchange(x):
        y = lax.all_to_all(x.reshape(groups, cap, -1), "ep", split_axis=0, concat_axis=0, tiled=True)
        return y.reshape(total, -1)

    sent_tok = jnp.dot(pick, tokens, preferred_element_type=F32).astype(BF16)
    own_tok = exchange(sent_tok)
    cot = jnp.dot(pick, cotangent, preferred_element_type=F32)
    sent_cot = (cot * slot_gate).astype(BF16)
    own_cot = exchange(sent_cot)

    def both(own, other):
        return jnp.where(
            core == 0,
            jnp.concatenate([own, other], axis=1),
            jnp.concatenate([other, own], axis=1),
        )

    w_in = jnp.concatenate([w_gate[0], w_up[0]], axis=1)
    hid = w_gate.shape[2]
    w_mine = lax.dynamic_slice_in_dim(w_in, core * half, half, 0)
    w_other = lax.dynamic_slice_in_dim(w_in, (1 - core) * half, half, 0)
    d_mine = lax.dynamic_slice_in_dim(w_down[0], core * half, half, 1)
    d_other = lax.dynamic_slice_in_dim(w_down[0], (1 - core) * half, half, 1)

    other_tok = lax.ppermute(own_tok, "tp", swap)
    rows_in = both(own_tok, other_tok)
    pre = jnp.dot(rows_in, w_in, preferred_element_type=F32)
    other_cot = lax.ppermute(own_cot, "tp", swap)
    grad_mine = lax.dot_general(own_cot, d_mine, LAST, preferred_element_type=F32)
    hidden_grad = grad_mine + lax.dot_general(other_cot, d_other, LAST, preferred_element_type=F32)
    gate_pre, up_pre = pre[:, :hid], pre[:, hid:]
    sigma = jax.nn.sigmoid(gate_pre)
    active = gate_pre * sigma
    hidden = (active * up_pre).astype(BF16)
    product_part = jnp.sum(hidden.astype(F32) * hidden_grad, axis=1)
    grads = jnp.concatenate(
        [
            (hidden_grad * up_pre * sigma * (1.0 + gate_pre * (1.0 - sigma))).astype(BF16),
            (hidden_grad * active).astype(BF16),
        ],
        axis=1,
    )
    part_other = lax.dot_general(grads, w_other, LAST, preferred_element_type=F32).astype(BF16)
    arrived = lax.ppermute(part_other, "tp", swap)
    part_mine = lax.dot_general(grads, w_mine, LAST, preferred_element_type=F32)
    row_grads = (part_mine + arrived.astype(F32)).astype(BF16)
    high = product_part.astype(BF16)
    low = (product_part - high.astype(F32)).astype(BF16)
    lane = lax.broadcasted_iota(jnp.int32, (total, 128), 1)
    spare = jnp.where(lane == 0, high[:, None], jnp.where(lane == 1, low[:, None], jnp.zeros((), BF16)))
    row_grads = jnp.concatenate([row_grads, spare], axis=1)
    back = exchange(row_grads)

    rows_in, grads, other_cot, hidden, row_grads = lax.optimization_barrier(
        (rows_in, grads, other_cot, hidden, row_grads)
    )
    gate_sum = lax.dot_general(rows_in, grads[:, :hid], ROWS, preferred_element_type=F32)
    up_sum = lax.dot_general(rows_in, grads[:, hid:], ROWS, preferred_element_type=F32)
    rows_cot = both(own_cot, other_cot)
    down_sum = lax.dot_general(hidden, rows_cot, ROWS, preferred_element_type=F32)
    in_norms = jnp.stack([jnp.sum(gate_sum * gate_sum, axis=1), jnp.sum(up_sum * up_sum, axis=1)])
    down_norms = jnp.sum(down_sum * down_sum, axis=1)
    in_norms = in_norms + lax.ppermute(in_norms, "tp", swap)
    pair = lax.dot_general(
        back[:, half:], jnp.concatenate([match[k] for k in range(top)], axis=1).astype(BF16), ROWS,
        preferred_element_type=F32,
    )
    route_products = (pair[0] + pair[1]).reshape(top, tok_rows)
    route_products = route_products + lax.ppermute(route_products, "tp", swap)
    gate_grad = (route_products.astype(BF16).astype(F32) / gate_t).T
    token_grad = lax.dot_general(pick, back[:, :half], ROWS, preferred_element_type=F32).astype(BF16)
    return (
        token_grad,
        gate_grad,
        gate_sum.astype(BF16)[None],
        up_sum.astype(BF16)[None],
        down_sum.astype(BF16)[None],
        in_norms[0][None],
        in_norms[1][None],
        down_norms[None],
    )


def solution(mesh):
    placed = (
        P("ep", "tp"),
        P("ep", "tp"),
        P("ep", None),
        P("ep", None),
        P("ep", None, "tp"),
        P("ep", None, "tp"),
        P("ep", "tp", None),
    )
    return jax.shard_map(
        per_device,
        mesh=mesh,
        in_specs=placed,
        out_specs=(
            P("ep", "tp"),
            P("ep", None),
            P("ep", None, "tp"),
            P("ep", None, "tp"),
            P("ep", "tp", None),
            P("ep", None),
            P("ep", None),
            P("ep", "tp"),
        ),
        check_vma=False,
    )
```

time: 410 us -> 325 us (0.79); the launches traced: 402 us -> 323 us
  blocking collectives: 96.9 us -> 0 us
  waiting for transfers between devices: 132 us -> 214 us
  local copies, waits for them, and re-layouts: 69.8 us -> 9.76 us
  between operations: 14.4 us -> 0.9 us
  matrix products: 59.8 us -> 65.8 us
    all_to_all x2 -> x0, blocking collectives: 92.9 us -> none  [the longest x1 82 us: per_device(): lax.all_to_all(sent_cot, 'ep', split_axis=0, concat_axis=0, tiled=True)]
    all_to_all x2 -> x3, waiting for transfers between devices: 125 us -> 209 us  [exchange(): lax.all_to_all(x.reshape(groups, cap, -1), 'ep', split_axis=0, concat_axi...]
    gather x5 -> x0, local copies, waits for them, and re-layouts: 40.8 us -> none  [the longest x2 14.6 us: per_device(): back_rows.reshape(-1, half_cols)[slot_of].astype(jnp.float32)]
    mul x5 -> x0, local copies, waits for them, and re-layouts: 11.8 us -> none  [the longest x3 11.5 us: per_device(): gate[:, :, None] * cotangent.astype(jnp.float32)[:, None, :]]
    select_n x2, other arithmetic: 0.03 us -> 8.14 us  [the longest x1 7.77 us: both(): jnp.where(core == 0, jnp.concatenate([own, other], axis=1), jnp.concatena...]
    reduce_sum x2 -> x1, other arithmetic: 8.5 us -> 0.92 us  [per_device(): jnp.sum(jnp.where(m, gate_t[k][None, :], 0.0), axis=1, keepdims=True)]
    all_gather x2 -> x0, waiting for transfers between devices: 6.68 us -> none  [the longest x1 6.66 us: per_device(): lax.all_gather(half_cot, 'tp', axis=2, tiled=True)]
    dot_general x8 -> x13, matrix products: 59.8 us -> 65.8 us  [the longest x1 11.1 us: per_device(): lax.dot_general(hidden, rows_cot, ROWS, preferred_element_type=F32)]
  transfers between devices with their start and end apart: 5 -> 8, of which waited for: 3 -> 4; matrix products, arithmetic and copies ran while one was open for 19% -> 20% of each run, Pallas kernels for 0% -> 0%
where the time goes in v1:
time: 325 us; the launch traced here: 323 us
  waiting for transfers between devices  214 us (66%)
  matrix products  65.8 us (20%)
  starting transfers between devices  18.3 us (6%)
  other arithmetic  14.4 us (4%)
  local copies, waits for them, and re-layouts  9.76 us (3%)
    all_to_all x3, waiting for transfers between devices, exchange(): lax.all_to_all(x.reshape(groups, cap, -1), 'ep', split_axis=0, concat_axi...  209 us
    all_to_all x3, starting transfers between devices, exchange(): lax.all_to_all(x.reshape(groups, cap, -1), 'ep', split_axis=0, concat_axi...  17.5 us
    dot_general x1, matrix products, per_device(): lax.dot_general(hidden, rows_cot, ROWS, preferred_element_type=F32)  11.1 us
    dot_general x1, matrix products, per_device(): pre = jnp.dot(rows_in, w_in, preferred_element_type=F32)  8.13 us
    select_n x1, other arithmetic, both(): jnp.where(core == 0, jnp.concatenate([own, other], axis=1), jnp.concatena...  7.77 us
    dot_general x1, matrix products, per_device(): lax.dot_general(other_cot, d_other, LAST, preferred_element_type=F32)  6.91 us
    unnamed x34, local copies, waits for them, and re-layouts  6.9 us
    dot_general x1, matrix products, per_device(): lax.dot_general(rows_in, grads[:, hid:], ROWS, preferred_element_type=F32)  6.62 us
  transfers between devices with their start and end apart: 8, of which 4 were waited for; matrix products, arithmetic and copies ran while one was open for 20% of the time, Pallas kernels for 0%

profile of v1, /device:TPU:14, one launch (start us, length us, event | category | flops | bytes accessed | tf_op | source)
XLA Modules:
  0.0 323.5 jit_solution(5678185878495180341)
XLA Ops:
  0.6 0.0 copy-start
  0.6 0.9 slice_reduce_fusion.3
  1.5 0.2 select_reduce_fusion.3
  1.7 0.8 slice_reduce_fusion
  2.5 0.8 add_reduce_fusion.1
  3.3 0.9 select_reduce_fusion
  4.2 0.0 copy-start.5
  4.2 5.4 %convolution_convert_fusion.1 = bf16[1152,1536]{1,0:T(8,128)(2,1)} fusion(bf16[1152,384]{1,0:T(8,128)(2,1)S(1)} %get-tuple-element.14, bf16[384,1536]{1,0:T(8,128)(2,1)} %param.7), kind=kOutput, calls=%fused_computation.3 | convolution fusion | flops 1360723968 | bytes 5603328 | tf_op jit(solution)/shard_map/dot_general | solution.py:49
  9.6 7.2 %all-to-all-start.1 = ((bf16[16,72,1536]{2,1,0:T(8,128)(2,1)}), bf16[16,72,1536]{2,1,0:T(8,128)(2,1)}, u32[]{:S(2)}, u32[]{:S(2)}) async-start(bf16[16,72,1536]{2,1,0:T(8,128)(2,1)} %bitcast.44), calls=%async_computation.1 | async-start | bytes 7077888 | tf_op jit(solution)/shard_map/all_to_all | solution.py:46
  16.8 5.1 %fusion = bf16[1152,1536]{1,0:T(8,128)(2,1)} fusion(bf16[1152,384]{1,0:T(8,128)(2,1)S(1)} %get-tuple-element.14, bf16[384,1536]{1,0:T(8,128)(2,1)} %param.8, f32[1152]{0:T(1024)S(1)} %reduce.6), kind=kOutput, calls=%fused_computation.1 | convolution fusion | flops 1362493440 | bytes 5607936 | tf_op jit(solution)/shard_map/dot_general | solution.py:51
  21.9 74.7 %all-to-all-done.1 = bf16[16,72,1536]{2,1,0:T(8,128)(2,1)} async-done(((bf16[16,72,1536]{2,1,0:T(8,128)(2,1)}), bf16[16,72,1536]{2,1,0:T(8,128)(2,1)}, u32[]{:S(2)}, u32[]{:S(2)}) %all-to-all-start.1) | async-done | bytes 3538976 | tf_op jit(solution)/shard_map/all_to_all | solution.py:46
  96.6 5.1 %all-to-all-start = ((bf16[16,72,1536]{2,1,0:T(8,128)(2,1)}), bf16[16,72,1536]{2,1,0:T(8,128)(2,1)}, u32[]{:S(2)}, u32[]{:S(2)}) async-start(bf16[16,72,1536]{2,1,0:T(8,128)(2,1)} %bitcast.43), calls=%async_computation | async-start | bytes 7077888 | tf_op jit(solution)/shard_map/all_to_all | solution.py:46
  101.7 0.1 collective-permute-start.1
  101.8 78.3 %all-to-all-done = bf16[16,72,1536]{2,1,0:T(8,128)(2,1)} async-done(((bf16[16,72,1536]{2,1,0:T(8,128)(2,1)}), bf16[16,72,1536]{2,1,0:T(8,128)(2,1)}, u32[]{:S(2)}, u32[]{:S(2)}) %all-to-all-start) | async-done | bytes 3538976 | tf_op jit(solution)/shard_map/all_to_all | solution.py:46
  180.1 0.0 collective-permute-start
  180.1 4.9 %fusion.27 = f32[1152,384]{0,1:T(8,128)} fusion(bf16[1152,1536]{1,0:T(8,128)(2,1)} %bitcast.3, bf16[1,384,3072]{2,1,0:T(8,128)(2,1)S(1)} %copy-done, s32[]{:T(128)S(6)} %select_n.46), kind=kOutput, calls=%fused_computation.51 | convolution fusion | flops 1358954496 | bytes 6488068 | tf_op jit(solution)/shard_map/dot_general | solution.py:73
  185.0 0.0 collective-permute-done.1
  185.0 7.8 %maximum_select_fusion = bf16[1152,3072]{1,0:T(8,128)(2,1)S(1)} fusion(bf16[1152,1536]{1,0:T(8,128)(2,1)} %collective-permute-done.1, bf16[1152,1536]{1,0:T(8,128)(2,1)} %bitcast.7, pred[]{:T(512)S(6)} %eq.70), kind=kLoop, calls=%fused_computation.4 | loop fusion | flops 31850496 | bytes 14155777 | tf_op jit(solution)/shard_map/jit(_where)/select_n | solution.py:56
  192.8 8.1 %fusion.8 = f32[1152,768]{0,1:T(8,128)} fusion(bf16[1152,3072]{1,0:T(8,128)(2,1)S(1)} %maximum_select_fusion, bf16[3072,384]{1,0:T(8,128)(2,1)S(1)} %bitcast.52, bf16[3072,384]{1,0:T(8,128)(2,1)S(1)} %bitcast.55), kind=kOutput, calls=%fused_computation.19 | convolution fusion | flops 5445255168 | bytes 15335424 | tf_op jit(solution)/shard_map/dot_general | solution.py:71
  201.0 0.0 collective-permute-done
  201.0 6.9 %multiply_reduce_fusion.3 = (f32[1152]{0:T(1024)S(1)}, bf16[1152,384]{0,1:T(8,128)(2,1)}, bf16[1152,384]{0,1:T(8,128)(2,1)S(1)}, bf16[1152,384]{0,1:T(8,128)(2,1)S(1)}) fusion(f32[1152,768]{0,1:T(8,128)} %fusion.8, f32[1152,384]{0,1:T(8,128)} %fusion.27, bf16[1152,1536]{1,0:T(8,128)(2,1)} %collective-permute-done, bf16[1,384,3072]{2,1,0:T(8,128)(2,1)S(1)} %copy-done, ...), kind=kOutput, calls=%fused_computation.39 | convolution fusion | flops 1367358336 | bytes 12685828 | tf_op jit(solution)/shard_map/dot_general | solution.py:74
  207.9 3.2 convolution_convert_fusion
  211.1 0.6 collective-permute-start.2
  211.7 0.4 select_select_fusion
  212.1 5.5 %collective-permute-done.2 = bf16[1152,1536]{1,0:T(8,128)(2,1)S(1)} collective-permute-done((bf16[1152,1536]{1,0:T(8,128)(2,1)S(1)}, bf16[1152,1536]{1,0:T(8,128)(2,1)S(1)}, u32[]{:S(2)}, u32[]{:S(2)}) %collective-permute-start.2) | collective-permute-done | bytes 3538976 | tf_op jit(solution)/shard_map/ppermute | solution.py:88
  217.5 3.3 %add_convert_fusion = bf16[1152,1536]{1,0:T(8,128)(2,1)S(1)} fusion(bf16[1152,1536]{1,0:T(8,128)(2,1)S(1)} %collective-permute-done.2, s32[]{:T(128)S(6)} %select_n.46, bf16[3072,384]{1,0:T(8,128)(2,1)S(1)} %bitcast.57, bf16[3072,384]{1,0:T(8,128)(2,1)S(1)} %bitcast.54, bf16[1152,384]{0,1:T(8,128)(2,1)S(1)} %get-tuple-element.57, ...), kind=kOutput, calls=%fused_computation.12 | convolution fusion | flops 2731474944 | bytes 13565956 | tf_op jit(solution)/shard_map/dot_general | solution.py:89
  220.8 2.2 pad_maximum_fusion.2
  223.0 5.2 %all-to-all-start.2 = ((bf16[16,72,1664]{2,1,0:T(8,128)(2,1)}), bf16[16,72,1664]{2,1,0:T(8,128)(2,1)}, u32[]{:S(2)}, u32[]{:S(2)}) async-start(bf16[16,72,1664]{2,1,0:T(8,128)(2,1)} %bitcast.40), calls=%async_computation.2 | async-start | bytes 7667712 | tf_op jit(solution)/shard_map/all_to_all | solution.py:46
  228.3 1.5 iota_compare_fusion
  229.7 0.1 pad_maximum_fusion.3
  229.9 0.0 slice-start.1
  229.9 6.6 %multiply_reduce_fusion.1 = (f32[3072]{0:T(1024)S(1)}, bf16[1,3072,384]{1,2,0:T(8,128)(2,1)S(1)}) fusion(bf16[1152,3072]{1,0:T(8,128)(2,1)} %copy-done.2, bf16[1152,768]{0,1:T(8,128)(2,1)S(1)} %pad_maximum_fusion.3), kind=kOutput, calls=%fused_computation.21 | convolution fusion | flops 2721444864 | bytes 10334208 | tf_op jit(solution)/shard_map/dot_general | solution.py:102
  236.6 0.0 copy-start.13
  236.6 4.6 %multiply_reduce_fusion.2 = (f32[3072]{0:T(1024)S(1)}, bf16[1,3072,384]{1,2,0:T(8,128)(2,1)}) fusion(bf16[1152,3072]{1,0:T(8,128)(2,1)S(1)} %bitcast.42, bf16[1152,768]{0,1:T(8,128)(2,1)S(1)} %pad_maximum_fusion.3), kind=kOutput, calls=%fused_computation.22 | convolution fusion | flops 2721444864 | bytes 10334208 | tf_op jit(solution)/shard_map/dot_general | solution.py:101
  241.2 0.1 collective-permute-start.4
  241.3 11.1 %multiply_reduce_fusion = (f32[384]{0:T(512)S(1)}, bf16[1,384,3072]{2,1,0:T(8,128)(2,1)}) fusion(bf16[1152,384]{0,1:T(8,128)(2,1)S(1)} %copy-done.13, bf16[1152,1536]{1,0:T(8,128)(2,1)} %collective-permute-done, bf16[1152,1536]{1,0:T(8,128)(2,1)} %bitcast.3, pred[]{:T(512)S(6)} %eq.70), kind=kOutput, calls=%fused_computation.20 | convolution fusion | flops 2753297920 | bytes 10323457 | tf_op jit(solution)/shard_map/dot_general | solution.py:104
  252.3 0.6 broadcast_in_dim.75
  252.9 2.4 copy.20
  255.3 4.4 %copy.19 = bf16[1,3072,384]{2,1,0:T(8,128)(2,1)} copy(bf16[1,3072,384]{1,2,0:T(8,128)(2,1)} %get-tuple-element.61) | data formatting | bytes 4718592
  259.8 0.6 fusion.51
  260.4 55.9 %all-to-all-done.2 = bf16[16,72,1664]{2,1,0:T(8,128)(2,1)} async-done(((bf16[16,72,1664]{2,1,0:T(8,128)(2,1)}), bf16[16,72,1664]{2,1,0:T(8,128)(2,1)}, u32[]{:S(2)}, u32[]{:S(2)}) %all-to-all-start.2) | async-done | bytes 3833888 | tf_op jit(solution)/shard_map/all_to_all | solution.py:46
  316.3 1.6 fusion.11
  317.9 0.0 copy-start.1
  317.9 0.0 copy-start.9
  317.9 0.1 collective-permute-start.3
  318.0 4.9 %fusion.15 = bf16[384,1536]{1,0:T(8,128)(2,1)} fusion(bf16[1152,384]{1,0:T(8,128)(2,1)S(1)} %copy-done.6, bf16[1152,1664]{1,0:T(8,128)(2,1)} %bitcast.11), kind=kOutput, calls=%fused_computation.31 | convolution fusion | flops 1359544320 | bytes 5603328 | tf_op jit(solution)/shard_map/dot_general | solution.py:115
  322.9 0.0 collective-permute-done.3
  322.9 0.6 fusion.40
  (39 shorter events, 0.2 us)
Async XLA Ops:
  0.6 179.4 %copy-start = (bf16[1,384,3072]{2,1,0:T(8,128)(2,1)S(1)}, bf16[1,384,3072]{2,1,0:T(8,128)(2,1)}, u32[]{:S(2)}) copy-start(bf16[1,384,3072]{2,1,0:T(8,128)(2,1)} %param.13) | copy-start | bytes 7077892
  4.2 12.6 %copy-start.5 = (bf16[1152,384]{1,0:T(8,128)(2,1)}, bf16[1152,384]{1,0:T(8,128)(2,1)S(1)}, u32[]{:S(2)}) copy-start(bf16[1152,384]{1,0:T(8,128)(2,1)S(1)} %get-tuple-element.14) | copy-start | bytes 2654212
  9.6 87.0 %all-to-all-start.1 = ((bf16[16,72,1536]{2,1,0:T(8,128)(2,1)}), bf16[16,72,1536]{2,1,0:T(8,128)(2,1)}, u32[]{:S(2)}, u32[]{:S(2)}) async-start(bf16[16,72,1536]{2,1,0:T(8,128)(2,1)} %bitcast.44), calls=%async_computation.1 | async-start | bytes 7077888 | tf_op jit(solution)/shard_map/all_to_all | solution.py:46
  96.6 83.5 %all-to-all-start = ((bf16[16,72,1536]{2,1,0:T(8,128)(2,1)}), bf16[16,72,1536]{2,1,0:T(8,128)(2,1)}, u32[]{:S(2)}, u32[]{:S(2)}) async-start(bf16[16,72,1536]{2,1,0:T(8,128)(2,1)} %bitcast.43), calls=%async_computation | async-start | bytes 7077888 | tf_op jit(solution)/shard_map/all_to_all | solution.py:46
  101.7 83.3 %collective-permute-start.1 = (bf16[1152,1536]{1,0:T(8,128)(2,1)}, bf16[1152,1536]{1,0:T(8,128)(2,1)}, u32[]{:S(2)}, u32[]{:S(2)}) collective-permute-start(bf16[1152,1536]{1,0:T(8,128)(2,1)} %bitcast.7), channel_id=1, source_target_pairs={{0,1},{1,0},{2,3},{3,2},{4,5},{5,4},{6,7},{7,6},{8,9},{9,8},{10,11... | collective-permute-start | bytes 10616840 | tf_op jit(solution)/shard_map/ppermute | solution.py:69
  180.1 20.9 %collective-permute-start = (bf16[1152,1536]{1,0:T(8,128)(2,1)}, bf16[1152,1536]{1,0:T(8,128)(2,1)}, u32[]{:S(2)}, u32[]{:S(2)}) collective-permute-start(bf16[1152,1536]{1,0:T(8,128)(2,1)} %bitcast.3), channel_id=1, source_target_pairs={{0,1},{1,0},{2,3},{3,2},{4,5},{5,4},{6,7},{7,6},{8,9},{9,8},{10,11... | collective-permute-start | bytes 10616840 | tf_op jit(solution)/shard_map/ppermute | solution.py:72
  185.0 7.8 %copy-start.10 = (bf16[1,3072,384]{2,1,0:T(8,128)(2,1)S(1)}, bf16[1,3072,384]{2,1,0:T(8,128)(2,1)}, u32[]{:S(2)}) copy-start(bf16[1,3072,384]{2,1,0:T(8,128)(2,1)} %param.12) | copy-start | bytes 7077892
  185.0 7.8 %copy-start.11 = (bf16[1,3072,384]{2,1,0:T(8,128)(2,1)S(1)}, bf16[1,3072,384]{2,1,0:T(8,128)(2,1)}, u32[]{:S(2)}) copy-start(bf16[1,3072,384]{2,1,0:T(8,128)(2,1)} %param.11) | copy-start | bytes 7077892
  192.8 8.2 %copy-start.2 = (bf16[1152,3072]{1,0:T(8,128)(2,1)}, bf16[1152,3072]{1,0:T(8,128)(2,1)S(1)}, u32[]{:S(2)}) copy-start(bf16[1152,3072]{1,0:T(8,128)(2,1)S(1)} %maximum_select_fusion) | copy-start | bytes 21233668
  201.0 6.9 %copy-start.12 = (bf16[1,3072,384]{2,1,0:T(8,128)(2,1)S(1)}, bf16[1,3072,384]{2,1,0:T(8,128)(2,1)}, u32[]{:S(2)}) copy-start(bf16[1,3072,384]{2,1,0:T(8,128)(2,1)} %param.11) | copy-start | bytes 7077892
  207.9 9.7 %copy-start.3 = (bf16[1152,384]{0,1:T(8,128)(2,1)}, bf16[1152,384]{0,1:T(8,128)(2,1)S(1)}, u32[]{:S(2)}) copy-start(bf16[1152,384]{0,1:T(8,128)(2,1)S(1)} %get-tuple-element.57) | copy-start | bytes 2654212
  211.1 6.4 %collective-permute-start.2 = (bf16[1152,1536]{1,0:T(8,128)(2,1)S(1)}, bf16[1152,1536]{1,0:T(8,128)(2,1)S(1)}, u32[]{:S(2)}, u32[]{:S(2)}) collective-permute-start(bf16[1152,1536]{1,0:T(8,128)(2,1)S(1)} %convolution_convert_fusion), channel_id=1, source_target_pairs={{0,1},{1,0},{2,3},{3,2},{4,5},{5,4},{6,7},{7,6},{8,9},{9,8},{10,11... | collective-permute-start | bytes 10616840 | tf_op jit(solution)/shard_map/ppermute | solution.py:88
  223.0 6.7 %copy-start.4 = (bf16[1152,384]{0,1:T(8,128)(2,1)S(1)}, bf16[1152,384]{0,1:T(8,128)(2,1)}, u32[]{:S(2)}) copy-start(bf16[1152,384]{0,1:T(8,128)(2,1)} %copy-done.3) | copy-start | bytes 2654212
  223.0 93.3 %all-to-all-start.2 = ((bf16[16,72,1664]{2,1,0:T(8,128)(2,1)}), bf16[16,72,1664]{2,1,0:T(8,128)(2,1)}, u32[]{:S(2)}, u32[]{:S(2)}) async-start(bf16[16,72,1664]{2,1,0:T(8,128)(2,1)} %bitcast.40), calls=%async_computation.2 | async-start | bytes 7667712 | tf_op jit(solution)/shard_map/all_to_all | solution.py:46
  229.7 6.8 %slice-start = ((s8[7077888]{0:T(1024)(128)(4,1)}), s8[4194304]{0:T(1024)(128)(4,1)S(1)}, s32[]{:S(2)}) async-start(s8[7077888]{0:T(1024)(128)(4,1)} %bitcast.41), calls=%async_computation.3 | async-start | bytes 8388608
  229.9 6.7 %slice-start.1 = ((s8[7077888]{0:T(1024)(128)(4,1)}), s8[2883584]{0:T(1024)(128)(4,1)S(1)}, s32[]{:S(2)}) async-start(s8[7077888]{0:T(1024)(128)(4,1)} %bitcast.41), calls=%async_computation.4 | async-start | bytes 5767168
  236.6 4.7 %copy-start.13 = (bf16[1152,384]{0,1:T(8,128)(2,1)S(1)}, bf16[1152,384]{0,1:T(8,128)(2,1)}, u32[]{:S(2)}) copy-start(bf16[1152,384]{0,1:T(8,128)(2,1)} %get-tuple-element.18) | copy-start | bytes 2654212
  241.2 18.6 %collective-permute-start.4 = (f32[2,3072]{1,0:T(2,128)S(1)}, f32[2,3072]{1,0:T(2,128)S(1)}, u32[]{:S(2)}, u32[]{:S(2)}) collective-permute-start(f32[2,3072]{1,0:T(2,128)S(1)} %pad_maximum_fusion.4), channel_id=1, source_target_pairs={{0,1},{1,0},{2,3},{3,2},{4,5},{5,4},{6,7},{7,6},{8,9},{9,8},{10,11... | collective-permute-start | bytes 73736 | tf_op jit(solution)/shard_map/ppermute | solution.py:107
  255.3 61.0 %copy-start.7 = (pred[1152,384]{1,0:T(32,128)(4,1)S(1)}, pred[1152,384]{1,0:T(32,128)(4,1)}, u32[]{:S(2)}) copy-start(pred[1152,384]{1,0:T(32,128)(4,1)} %get-tuple-element.69) | copy-start | bytes 1327108
  255.3 61.0 %copy-start.8 = (pred[1152,384]{1,0:T(32,128)(4,1)S(1)}, pred[1152,384]{1,0:T(32,128)(4,1)}, u32[]{:S(2)}) copy-start(pred[1152,384]{1,0:T(32,128)(4,1)} %get-tuple-element.70) | copy-start | bytes 1327108
  255.3 62.7 %copy-start.6 = (bf16[1152,384]{1,0:T(8,128)(2,1)S(1)}, bf16[1152,384]{1,0:T(8,128)(2,1)}, u32[]{:S(2)}) copy-start(bf16[1152,384]{1,0:T(8,128)(2,1)} %copy-done.5) | copy-start | bytes 2654212
  317.9 5.6 %copy-start.1 = (bf16[1,384,3072]{2,1,0:T(8,128)(2,1)S(1)}, bf16[1,384,3072]{2,1,0:T(8,128)(2,1)}, u32[]{:S(2)}) copy-start(bf16[1,384,3072]{2,1,0:T(8,128)(2,1)} %param.13) | copy-start | bytes 7077892
  317.9 5.0 %copy-start.9 = (f32[384,2]{0,1:T(2,128)S(1)}, f32[384,2]{0,1:T(2,128)}, u32[]{:S(2)}) copy-start(f32[384,2]{0,1:T(2,128)} %param.10) | copy-start | bytes 9220
  317.9 5.0 %collective-permute-start.3 = (f32[2,384]{1,0:T(2,128)S(1)}, f32[2,384]{1,0:T(2,128)S(1)}, u32[]{:S(2)}, u32[]{:S(2)}) collective-permute-start(f32[2,384]{1,0:T(2,128)S(1)} %add.74), channel_id=1, source_target_pairs={{0,1},{1,0},{2,3},{3,2},{4,5},{5,4},{6,7},{7,6},{8,9},{9,8},{10,11... | collective-permute-start | bytes 9224 | tf_op jit(solution)/shard_map/ppermute | solution.py:113
